TPU v7x, 32 devices: a whole 2x2x4 slice. The times are simulated.
32 devices in a mesh: fs: 4 (over y, x), tp: 8 (over z, core).
Axes of the slice: x: 2, y: 2, z: 4, core: 2. Of those that a mesh axis runs over, the one named last changes fastest.
Arguments:
- saved_input: bfloat16 [4096, 4096], P('fs', 'tp'), may hold values from -6 to 6
- query_cot: bfloat16 [4096, 4096], P('fs', 'tp'), may hold values from -6 to 6
- key_cot: bfloat16 [4096, 4096], P('fs', 'tp'), may hold values from -6 to 6
- query_master: float32 [4096, 4096], P('fs', 'tp'), may hold values from -0.09375 to 0.09375
- key_master: float32 [4096, 4096], P('fs', 'tp'), may hold values from -0.09375 to 0.09375
- query_basis: bfloat16 [4096, 256], P('fs'), may hold values from -3 to 3
- key_basis: bfloat16 [4096, 256], P('fs'), may hold values from -3 to 3
- query_first: float32 [256, 4096], P('fs', 'tp'), may hold values from -240 to 240
- query_second: float32 [256, 4096], P('fs', 'tp'), may hold values from 1000 to 20000
- key_first: float32 [256, 4096], P('fs', 'tp'), may hold values from -240 to 240
- key_second: float32 [256, 4096], P('fs', 'tp'), may hold values from 1000 to 20000
Outputs:
- query_step: float32 [4096, 4096], P('fs', 'tp')
- query_weight: float32 [4096, 4096], P('fs', 'tp')
- query_copy: bfloat16 [4096, 4096], P(None, 'tp')
- query_first_new: float32 [256, 4096], P('fs', 'tp')
- query_second_new: float32 [256, 4096], P('fs', 'tp')
- key_step: float32 [4096, 4096], P('fs', 'tp')
- key_weight: float32 [4096, 4096], P('fs', 'tp')
- key_copy: bfloat16 [4096, 4096], P(None, 'tp')
- key_first_new: float32 [256, 4096], P('fs', 'tp')
- key_second_new: float32 [256, 4096], P('fs', 'tp')
All inputs are finite; a program needn't handle non-finite values.
Results may differ from a plain program's by a relative error of at most 0.0065.
Values may be sent and summed in bfloat16 or wider, within the bound.
A program may use at most 64 MiB of HBM per device.

v0:
```python
import functools

import jax
import jax.numpy as jnp
from jax import lax
from jax.experimental import pallas as pl
from jax.experimental.pallas import tpu as pltpu
from jax.sharding import PartitionSpec as P

HD = 128

moment_decay = 0.8
square_decay = 0.9
square_floor = 1.0
norm_floor = 0.01
step_rate = 0.01

BF = jnp.bfloat16
F32 = jnp.float32
MESH = pl.DeviceIdType.MESH


def exchange_kernel(
    fs,
    tp,
    x_hbm,
    qc_hbm,
    kc_hbm,
    qm_hbm,
    km_hbm,
    qb_hbm,
    kb_hbm,
    qf_ref,
    qs_ref,
    kf_ref,
    ks_ref,
    qfn_ref,
    qsn_ref,
    kfn_ref,
    ksn_ref,
    ratio_ref,
    scale_ref,
    gathered,
    basis_out,
    basis,
    x_v,
    cot,
    master,
    rounded,
    half_send,
    half_recv,
    half_own,
    z_send,
    z_recv,
    low,
    proj,
    proj_send,
    proj_recv,
    load_sem,
    b_send,
    b_recv,
    d_send,
    d_recv,
    p_send,
    p_recv,
    zr_send,
    zr_recv,
    zg_send,
    zg_recv,
    pf_send,
    pf_recv,
    rs_send,
    rs_recv,
    ag_send,
    ag_recv,
    m_send,
    m_recv,
    out_sem,
):
    f = lax.axis_index("fs")
    t = lax.axis_index("tp")
    z, c = t // 2, t % 2
    depth = tp // 2
    relay = fs == 4
    rows, rank = qb_hbm.shape
    width = qc_hbm.shape[1]
    tokens, columns = x_v.shape
    part = rank // fs
    half_rows = rows // 2
    half = tokens // 2
    chunk = tokens // tp

    def at(start, size):
        return pl.ds(pl.multiple_of(start, size), size)

    def remote(src, dst, send, recv, df, dt):
        return pltpu.make_async_remote_copy(
            src_ref=src,
            dst_ref=dst,
            send_sem=send,
            recv_sem=recv,
            device_id=(df, dt),
            device_id_type=MESH,
        )

    loads = [
        pltpu.make_async_copy(qb_hbm, basis.at[0, at(f * rows, rows)], load_sem.at[0]),
        pltpu.make_async_copy(kb_hbm, basis.at[1, at(f * rows, rows)], load_sem.at[1]),
        pltpu.make_async_copy(qm_hbm, master.at[0], load_sem.at[2]),
        pltpu.make_async_copy(km_hbm, master.at[1], load_sem.at[3]),
        pltpu.make_async_copy(x_hbm, x_v, load_sem.at[4]),
        pltpu.make_async_copy(qc_hbm, cot.at[0], load_sem.at[5]),
        pltpu.make_async_copy(kc_hbm, cot.at[1], load_sem.at[6]),
    ]
    for load in loads:
        load.start()

    barrier = pltpu.get_barrier_semaphore()
    for m in range(1, fs):
        pl.semaphore_signal(barrier, inc=1, device_id=(f ^ m, t), device_id_type=MESH)
    pl.semaphore_signal(barrier, inc=1, device_id=(f, t ^ 1), device_id_type=MESH)
    for d in range(1, depth):
        other = lax.rem(z + d, depth) * 2 + c
        pl.semaphore_signal(barrier, inc=1, device_id=(f, other), device_id_type=MESH)
    loads[0].wait()
    loads[1].wait()
    pl.semaphore_wait(barrier, fs - 1 + depth)

    def basis_copy(j, m, owner, target):
        piece = basis.at[j, at(owner * rows + c * half_rows, half_rows)]
        return remote(piece, piece, b_send.at[m, j], b_recv.at[m, j], target, t)

    direct = [m for m in range(1, fs) if not (relay and m == 3)]
    basis_copies = {}
    for m in direct:
        for j in (0, 1) if m % 2 else (1, 0):
            basis_copies[m, j] = basis_copy(j, m, f, f ^ m)
            basis_copies[m, j].start()

    loads[2].wait()
    loads[3].wait()
    tile = min(rows, 128)

    for j in range(2):

        @pl.loop(0, rows // tile)
        def _(i, j=j):
            place = at(i * tile, tile)
            rounded[j, place, :] = master[j, place, :].astype(BF)

    def master_copy(j, m):
        return remote(
            rounded.at[j],
            gathered.at[j, at(f * rows, rows)],
            m_send.at[m, j],
            m_recv.at[m, j],
            f ^ m,
            t,
        )

    def master_relay(j, side):
        source = 1 + j
        piece = gathered.at[j, at((f ^ source) * rows + side * half_rows, half_rows)]
        slot = 3 + side
        return remote(piece, piece, m_send.at[slot, j], m_recv.at[slot, j], f ^ (2 - j), t)

    if relay:
        basis_copies[1, 0].wait_recv()
        basis_copies[3, 0] = basis_copy(0, 3, f ^ 1, f ^ 2)
        basis_copies[3, 0].start()
        basis_copies[2, 1].wait_recv()
        basis_copies[3, 1] = basis_copy(1, 3, f ^ 2, f ^ 1)
        basis_copies[3, 1].start()

    master_copies = {}
    for turn in range(2):
        for m in direct:
            j = (m + 1 + turn) % 2
            master_copies[m, j] = master_copy(j, m)
            master_copies[m, j].start()
    kept = pltpu.make_async_copy(rounded, gathered.at[:, at(f * rows, rows)], out_sem.at[1])
    kept.start()

    waited = {(1, 0), (2, 1)} if relay else set()
    for m in range(1, fs):
        for j in range(2):
            if (m, j) not in waited:
                basis_copies[m, j].wait_recv()

    loads[4].wait()
    step = min(half, 256)

    def project(start, j):
        return jnp.dot(
            x_v[at(start, step), :],
            basis[j, at(t * columns, columns), :],
            preferred_element_type=F32,
        )

    for j in range(2):

        @pl.loop(0, half // step)
        def _(i, j=j):
            half_send[at(i * step, step), j * rank : (j + 1) * rank] = project(
                (1 - c) * half + i * step, j
            ).astype(BF)

    swap = remote(half_send, half_recv, p_send, p_recv, f, t ^ 1)
    swap.start()
    for j in range(2):

        @pl.loop(0, half // step)
        def _(i, j=j):
            half_own[at(i * step, step), j * rank : (j + 1) * rank] = project(
                c * half + i * step, j
            )

    swap.wait_recv()

    partner_copies = []
    for m in range(1, fs):
        piece = basis.at[:, at((f ^ m) * rows + c * half_rows, half_rows)]
        copy = remote(piece, piece, d_send.at[m], d_recv.at[m], f, t ^ 1)
        copy.start()
        partner_copies.append(copy)

    @pl.loop(0, half // chunk)
    def _(i):
        place = at(i * chunk, chunk)
        both = half_own[place, :] + half_recv[place, :].astype(F32)
        half_own[place, :] = both
        z_send[place, :] = both.astype(BF)

    z_copies = []
    for d in range(1, depth):
        other = lax.rem(z + d, depth)
        copy = remote(
            z_send.at[at(other * chunk, chunk)],
            z_recv.at[d],
            zr_send.at[d],
            zr_recv.at[d],
            f,
            other * 2 + c,
        )
        copy.start()
        z_copies.append(copy)
    total = half_own[at(z * chunk, chunk), :]
    for d in range(1, depth):
        z_copies[d - 1].wait_recv()
        total = total + z_recv[d].astype(F32)
    low[at(c * half + z * chunk, chunk), :] = total.astype(BF)

    def low_piece(d, core):
        return low.at[at(core * half + lax.rem(z + depth - d, depth) * chunk, chunk)]

    g_copies = []
    for d in range(1, depth):
        other = lax.rem(z + d, depth)
        copy = remote(
            low_piece(0, c), low_piece(0, c), zg_send.at[d], zg_recv.at[d], f, other * 2 + c
        )
        copy.start()
        g_copies.append(copy)
    forwards = []
    for d in range(depth):
        if d > 0:
            g_copies[d - 1].wait_recv()
        copy = remote(low_piece(d, c), low_piece(d, c), pf_send.at[d], pf_recv.at[d], f, t ^ 1)
        copy.start()
        forwards.append(copy)
    loads[5].wait()
    loads[6].wait()
    for copy in forwards:
        copy.wait_recv()

    for j in range(2):
        product = lax.dot_general(
            low[:, j * rank : (j + 1) * rank],
            cot[j],
            (((0,), (0,)), ((), ())),
            preferred_element_type=F32,
        )
        proj[j] = product
        proj_send[j] = product.astype(BF)
    r_copies = []
    for m in range(1, fs):
        copy = remote(
            proj_send.at[:, at((f ^ m) * part, part)],
            proj_recv.at[m],
            rs_send.at[m],
            rs_recv.at[m],
            f ^ m,
            t,
        )
        copy.start()
        r_copies.append(copy)
    if relay:
        for j in range(2):
            master_copies[1 + j, j].wait_recv()
            master_copies[3, j] = master_relay(j, 0)
            master_copies[3, j].start()
    for copy in r_copies:
        copy.wait_recv()

    own = at(f * part, part)
    moments = ((qf_ref, qs_ref, qfn_ref, qsn_ref), (kf_ref, ks_ref, kfn_ref, ksn_ref))
    for j, (first, second, first_out, second_out) in enumerate(moments):
        summed = proj[j, own, :]
        for m in range(1, fs):
            summed = summed + proj_recv[m, j].astype(F32)
        first_new = moment_decay * first[...] + (1.0 - moment_decay) * summed
        second_new = square_decay * second[...] + (1.0 - square_decay) * summed * summed
        first_out[...] = first_new
        second_out[...] = second_new
        ratio_ref[j, own, :] = (first_new / jnp.sqrt(second_new + square_floor)).astype(BF)

    a_copies = []
    for m in range(1, fs):
        piece = ratio_ref.at[:, own]
        copy = remote(piece, piece, ag_send.at[m], ag_recv.at[m], f ^ m, t)
        copy.start()
        a_copies.append(copy)

    if relay:
        for j in range(2):
            master_copies[4, j] = master_relay(j, 1)
            master_copies[4, j].start()

    for copy in partner_copies:
        copy.wait_recv()
    store = pltpu.make_async_copy(basis, basis_out, out_sem.at[0])
    store.start()
    for copy in a_copies:
        copy.wait_recv()

    high = min(rows, 256)
    for j in range(2):

        def add(i, total, j=j):
            update = jnp.dot(
                basis[j, at(i * high, high), :], ratio_ref[j], preferred_element_type=F32
            )
            return total + jnp.sum((update * update).reshape(high // 8, 8, width), axis=0)

        sums = lax.fori_loop(0, fs * rows // high, add, jnp.zeros((8, width), F32))
        sums = jnp.sum(sums, axis=0, keepdims=True)
        for h in range(width // HD):
            head = slice(h * HD, (h + 1) * HD)
            total = jnp.sum(sums[:, head], axis=1, keepdims=True)
            scale = 1.0 / jnp.sqrt(total / (fs * rows * HD) + norm_floor)
            scale_ref[j, :, head] = jnp.broadcast_to(scale, (8, HD))

    store.wait()
    kept.wait()
    early = {(1, 0), (2, 1)} if relay else set()
    for place, copy in master_copies.items():
        if place not in early:
            copy.wait_recv()
    for copy in list(basis_copies.values()) + partner_copies + [swap] + z_copies:
        copy.wait_send()
    for copy in g_copies + forwards + r_copies + a_copies + list(master_copies.values()):
        copy.wait_send()


def final_kernel(*refs):
    scale_ref, ratio_ref, basis_ref, gathered_ref = refs[:4]
    inputs, moments, outs, moments_out = refs[4:8], refs[8:12], refs[12:18], refs[18:]
    for j in range(2):
        scale = scale_ref[j, 0:1, :]
        own_basis, master = inputs[2 * j : 2 * j + 2]
        step_out, weight_out, copy_out = outs[3 * j : 3 * j + 3]
        update = jnp.dot(own_basis[...], ratio_ref[j], preferred_element_type=F32)
        step = update * scale
        step_out[...] = step
        weight_out[...] = master[...] - step_rate * step
        update = jnp.dot(basis_ref[j], ratio_ref[j], preferred_element_type=F32)
        step = update * scale
        copy_out[...] = (gathered_ref[j].astype(F32) - step_rate * step).astype(BF)

    @pl.when(pl.program_id(0) == 0)
    def _():
        for source, target in zip(moments, moments_out):
            target[...] = source[...]


def body(fs, tp, *args):
    saved_input, query_cot, _, query_master, key_master, query_basis, key_basis = args[:7]
    rows, rank = query_basis.shape
    tokens, columns = saved_input.shape
    width = query_cot.shape[1]
    part = rank // fs
    depth = tp // 2
    count = fs * rows
    half, chunk = tokens // 2, tokens // tp
    any_spec = pl.BlockSpec(memory_space=pl.ANY)
    vmem = pl.BlockSpec(memory_space=pltpu.VMEM)
    dma = pltpu.SemaphoreType.DMA
    moment = jax.ShapeDtypeStruct((part, width), F32)
    pairs = []
    for shape in ((fs, 2), (fs,), (), (depth,), (depth,), (depth,), (fs,), (fs,), (fs + 1, 2)):
        pairs += [dma(shape), dma(shape)]
    results = pl.pallas_call(
        functools.partial(exchange_kernel, fs, tp),
        name="exchange",
        out_shape=(
            moment,
            moment,
            moment,
            moment,
            jax.ShapeDtypeStruct((2, rank, width), BF),
            jax.ShapeDtypeStruct((2, 8, width), F32),
            jax.ShapeDtypeStruct((2, count, width), BF),
            jax.ShapeDtypeStruct((2, count, rank), BF),
        ),
        in_specs=[any_spec] * 7 + [vmem] * 4,
        out_specs=(vmem,) * 6 + (any_spec,) * 2,
        scratch_shapes=[
            pltpu.VMEM((2, count, rank), BF),
            pltpu.VMEM((tokens, columns), BF),
            pltpu.VMEM((2, tokens, width), BF),
            pltpu.VMEM((2, rows, width), F32),
            pltpu.VMEM((2, rows, width), BF),
            pltpu.VMEM((half, 2 * rank), BF),
            pltpu.VMEM((half, 2 * rank), BF),
            pltpu.VMEM((half, 2 * rank), F32),
            pltpu.VMEM((half, 2 * rank), BF),
            pltpu.VMEM((depth, chunk, 2 * rank), BF),
            pltpu.VMEM((tokens, 2 * rank), BF),
            pltpu.VMEM((2, rank, width), F32),
            pltpu.VMEM((2, rank, width), BF),
            pltpu.VMEM((fs, 2, part, width), BF),
            dma((7,)),
            *pairs,
            dma((2,)),
        ],
        compiler_params=pltpu.CompilerParams(
            collective_id=0, has_side_effects=True, vmem_limit_bytes=60 * 1024 * 1024
        ),
    )(*args)
    moments, (ratio, scale, gathered, basis) = results[:4], results[4:]

    steps = min(8, rows // 16)
    own_tile, tile = rows // steps, count // steps

    def row(i):
        return (i, 0)

    def pair(i):
        return (0, i, 0)

    def whole(i):
        return (0, 0, 0)

    own_spec = pl.BlockSpec((own_tile, width), row)
    full_spec = pl.BlockSpec((tile, width), row)
    basis_spec = pl.BlockSpec((own_tile, rank), row)
    moment_spec = pl.BlockSpec((part, width), lambda i: (0, 0))
    big = jax.ShapeDtypeStruct((rows, width), F32)
    copied = jax.ShapeDtypeStruct((count, width), BF)
    outs = pl.pallas_call(
        final_kernel,
        name="final",
        out_shape=(big, big, copied) * 2 + (moment,) * 4,
        grid=(steps,),
        in_specs=[
            pl.BlockSpec((2, 8, width), whole),
            pl.BlockSpec((2, rank, width), whole),
            pl.BlockSpec((2, tile, rank), pair),
            pl.BlockSpec((2, tile, width), pair),
            basis_spec,
            own_spec,
            basis_spec,
            own_spec,
        ]
        + [moment_spec] * 4,
        out_specs=(own_spec, own_spec, full_spec) * 2 + (moment_spec,) * 4,
        compiler_params=pltpu.CompilerParams(vmem_limit_bytes=60 * 1024 * 1024),
    )(scale, ratio, basis, gathered, query_basis, query_master, key_basis, key_master, *moments)
    return (*outs[:3], *outs[6:8], *outs[3:6], *outs[8:])


def solution(mesh):
    split, tall, wide = P("fs", "tp"), P("fs", None), P(None, "tp")
    outs = (split, split, wide, split, split)
    return jax.shard_map(
        functools.partial(body, mesh.shape["fs"], mesh.shape["tp"]),
        mesh=mesh,
        in_specs=(split,) * 5 + (tall, tall) + (split,) * 4,
        out_specs=outs + outs,
        check_vma=False,
    )
```

profile of v0, /device:TPU:0, one launch (start us, length us, event | category | flops | bytes accessed | tf_op | source)
XLA Modules:
  0.0 122.0 jit_solution(10342961896515980029)
XLA Ops:
  0.6 105.7 %exchange.1 = (f32[64,512]{1,0:T(8,128)}, f32[64,512]{1,0:T(8,128)}, f32[64,512]{1,0:T(8,128)}, f32[64,512]{1,0:T(8,128)}, bf16[2,256,512]{2,1,0:T(8,128)(2,1)},...) custom-call(bf16[1024,512]{1,0:T(8,128)(2,1)} %x_hbm.1, ...), custom_call_target="tpu_custom_call" | custom-call | tf_op jit(solution)/shard_map/exchange/pallas_call | solution.py:402
  106.3 15.6 %final.1 = (f32[1024,512]{1,0:T(8,128)}, f32[1024,512]{1,0:T(8,128)}, bf16[4096,512]{1,0:T(8,128)(2,1)}, f32[1024,512]{1,0:T(8,128)}, f32[1024,512]{1,0:T(8,128)...) custom-call(f32[2,8,512]{2,1,0:T(8,128)} %get-tuple-element.28.refs_, ...), custom_call_target="tpu_custom_call" | custom-call | tf_op jit(solution)/shard_map/final/pallas_call | solution.py:460
where the time goes:
time: 122 us
  Pallas kernels  121 us (99%)
    pallas_call x1, Pallas kernels, body(): pl.pallas_call(functools.partial(exchange_kernel, fs, tp), name='exchange...  106 us
    pallas_call x1, Pallas kernels, body(): pl.pallas_call(final_kernel, name='final', out_shape=(big, big, copied) *...  15.6 us

commit v1 on v0

v1 whole, which is shorter than its diff:
```python
import functools

import jax
import jax.numpy as jnp
from jax import lax
from jax.experimental import pallas as pl
from jax.experimental.pallas import tpu as pltpu
from jax.sharding import PartitionSpec as P

HD = 128

moment_decay = 0.8
square_decay = 0.9
square_floor = 1.0
norm_floor = 0.01
step_rate = 0.01

BF = jnp.bfloat16
F32 = jnp.float32
MESH = pl.DeviceIdType.MESH


def exchange_kernel(
    fs,
    tp,
    x_hbm,
    qc_hbm,
    kc_hbm,
    qm_hbm,
    km_hbm,
    qb_hbm,
    kb_hbm,
    qf_hbm,
    qs_hbm,
    kf_hbm,
    ks_hbm,
    first_new,
    second_new,
    step_ref,
    weight_ref,
    copy_ref,
    basis,
    gathered,
    x_v,
    cot,
    master,
    moment,
    half_send,
    half_recv,
    half_own,
    z_send,
    z_recv,
    low,
    proj,
    proj_send,
    proj_recv,
    ratio,
    sums,
    scales,
    load_sem,
    b_send,
    b_recv,
    d_send,
    d_recv,
    p_send,
    p_recv,
    zr_send,
    zr_recv,
    zg_send,
    zg_recv,
    pf_send,
    pf_recv,
    g_send,
    g_recv,
    gp_send,
    gp_recv,
    rs_send,
    rs_recv,
    ag_send,
    ag_recv,
    s_send,
    s_recv,
    m_send,
    m_recv,
    r_send,
    r_recv,
):
    f = lax.axis_index("fs")
    t = lax.axis_index("tp")
    z, c = t // 2, t % 2
    depth = tp // 2
    relay = fs == 4
    rows, rank = qb_hbm.shape
    width = qc_hbm.shape[1]
    tokens, columns = x_v.shape
    part = rank // fs
    half = tokens // 2
    chunk = tokens // tp
    group = rows // columns
    owner = t // group
    role = f ^ owner
    tile = min(rows, 128)
    pieces = rows // tile

    def at(start, size):
        return pl.ds(pl.multiple_of(start, size), size)

    def remote(src, dst, send, recv, df, dt):
        return pltpu.make_async_remote_copy(
            src_ref=src,
            dst_ref=dst,
            send_sem=send,
            recv_sem=recv,
            device_id=(df, dt),
            device_id_type=MESH,
        )

    own_rows = at(f * rows, rows)
    sources = (
        (qb_hbm, basis.at[0, own_rows]),
        (kb_hbm, basis.at[1, own_rows]),
        (qm_hbm, master.at[0]),
        (km_hbm, master.at[1]),
        (x_hbm, x_v),
        (qc_hbm, cot.at[0]),
        (kc_hbm, cot.at[1]),
        (qf_hbm, moment.at[0]),
        (qs_hbm, moment.at[1]),
        (kf_hbm, moment.at[2]),
        (ks_hbm, moment.at[3]),
    )
    loads = [
        pltpu.make_async_copy(source, target, load_sem.at[i])
        for i, (source, target) in enumerate(sources)
    ]
    for load in loads:
        load.start()

    barrier = pltpu.get_barrier_semaphore()
    for m in range(1, fs):
        pl.semaphore_signal(barrier, inc=1, device_id=(f ^ m, t), device_id_type=MESH)
    pl.semaphore_signal(barrier, inc=1, device_id=(f, t ^ 1), device_id_type=MESH)
    for d in range(1, depth):
        other = lax.rem(z + d, depth) * 2 + c
        pl.semaphore_signal(barrier, inc=1, device_id=(f, other), device_id_type=MESH)

    def master_copy(m, j, i):
        piece = gathered.at[j, at(f * rows + i * tile, tile)]
        return remote(piece, piece, m_send.at[m - 1], m_recv.at[m - 1, j, i], f ^ m, t)

    def relay_copy(m, i):
        piece = gathered.at[2 - m, at((f ^ (3 - m)) * rows + i * tile, tile)]
        return remote(piece, piece, r_send.at[m - 1], r_recv.at[m - 1, i], f ^ m, t)

    def issue(m, start, stop):
        for turn in range(2):
            j = (m + 1 + turn) % 2
            low_end, high_end = max(start, turn * pieces), min(stop, (turn + 1) * pieces)
            if low_end < high_end:

                @pl.loop(low_end - turn * pieces, high_end - turn * pieces)
                def _(i, j=j):
                    master_copy(m, j, i).start()

        low_end, high_end = max(start, 2 * pieces), min(stop, 3 * pieces)
        if low_end < high_end:

            @pl.loop(low_end - 2 * pieces, high_end - 2 * pieces)
            def _(i):
                master_copy(3 - m, 2 - m, i).wait_recv()
                relay_copy(m, i).start()

    def share(start, stop):
        for m in (1, 2):
            issue(m, start, stop)

    count = 3 * pieces
    marks = [count * k // 24 for k in MARKS]

    piece_rows = columns // 2

    def basis_copy(m, j, h, target):
        piece = basis.at[j, at(t * columns + h * piece_rows, piece_rows)]
        return remote(piece, piece, b_send.at[m, j, h], b_recv.at[j, h], target, t)

    loads[0].wait()
    loads[1].wait()
    pl.semaphore_wait(barrier, fs - 1 + depth)
    if relay:

        @pl.when(role == 0)
        def _():
            for j in range(2):
                basis_copy(0, j, 0, f ^ 1).start()
                basis_copy(0, j, 1, f ^ 2).start()
    else:

        @pl.when(role == 0)
        def _():
            for m in range(1, fs):
                for j in range(2):
                    for h in range(2):
                        basis_copy(m, j, h, f ^ m).start()

    for j in range(2):
        loads[2 + j].wait()

        @pl.loop(0, pieces)
        def _(i, j=j):
            gathered[j, at(f * rows + i * tile, tile), :] = master[j, at(i * tile, tile), :].astype(BF)

    if relay:
        first_marks = [[count * k // 24 for k in pair] for pair in FIRST]

        for k in range(4):

            @pl.when(role == k)
            def _(k=k):
                issue(1, 0, first_marks[k][0])
                issue(2, 0, first_marks[k][1])

        @pl.when(role == 1)
        def _():
            for j in range(2):
                basis_copy(0, j, 0, f ^ 2).wait_recv()
                basis_copy(0, j, 0, f ^ 2).start()

        @pl.when(role == 2)
        def _():
            for j in range(2):
                basis_copy(0, j, 1, f ^ 1).wait_recv()
                basis_copy(0, j, 1, f ^ 1).start()

        @pl.when(role == 3)
        def _():
            for j in range(2):
                basis_copy(0, j, 0, f ^ 1).wait_recv()
                basis_copy(0, j, 0, f ^ 1).start()
                basis_copy(0, j, 1, f ^ 2).wait_recv()
                basis_copy(0, j, 1, f ^ 2).start()

        for k in range(4):

            @pl.when(role == k)
            def _(k=k):
                issue(1, first_marks[k][0], marks[0])
                issue(2, first_marks[k][1], marks[0])
    else:
        for m in range(1, fs):
            for j in range(2):

                @pl.loop(0, pieces)
                def _(i, m=m, j=j):
                    master_copy(m, j, i).start()

    def basis_wait(j):
        if relay:

            @pl.when(role == 1)
            def _():
                basis_copy(0, j, 1, f).wait_recv()

            @pl.when(role == 2)
            def _():
                basis_copy(0, j, 0, f).wait_recv()
        else:

            @pl.when(role != 0)
            def _():
                for h in range(2):
                    basis_copy(0, j, h, f).wait_recv()

    def partner_copy(j):
        piece = basis.at[j, at(t * columns, columns)]
        return remote(piece, piece, d_send.at[j], d_recv.at[j], f, t ^ 1)

    step = min(half, 256)

    def project(start, j):
        return jnp.dot(
            x_v[at(start, step), :],
            basis[j, at(t * columns, columns), :],
            preferred_element_type=F32,
        )

    def swap(j):
        return remote(half_send.at[j], half_recv.at[j], p_send.at[j], p_recv.at[j], f, t ^ 1)

    def z_copy(j, d):
        other = lax.rem(z + d, depth)
        return remote(
            z_send.at[j, at(other * chunk, chunk)],
            z_recv.at[d, j],
            zr_send.at[j, d],
            zr_recv.at[j, d],
            f,
            other * 2 + c,
        )

    loads[4].wait()
    for j in range(2):
        basis_wait(j)

        @pl.loop(0, half // step)
        def _(i, j=j):
            half_send[j, at(i * step, step), :] = project((1 - c) * half + i * step, j).astype(BF)

        swap(j).start()

        @pl.loop(0, half // step)
        def _(i, j=j):
            half_own[j, at(i * step, step), :] = project(c * half + i * step, j)

        @pl.when(role != 0)
        def _(j=j):
            partner_copy(j).start()

        swap(j).wait_recv()

        @pl.loop(0, half // chunk)
        def _(i, j=j):
            place = at(i * chunk, chunk)
            both = half_own[j, place, :] + half_recv[j, place, :].astype(F32)
            half_own[j, place, :] = both
            z_send[j, place, :] = both.astype(BF)

        for d in range(1, depth):
            z_copy(j, d).start()

    def low_piece(j, d, core):
        return low.at[j, at(core * half + lax.rem(z + depth - d, depth) * chunk, chunk)]

    def g_copy(j, d):
        other = lax.rem(z + d, depth)
        return remote(
            low_piece(j, 0, c),
            low_piece(j, 0, c),
            zg_send.at[j, d],
            zg_recv.at[j, d],
            f,
            other * 2 + c,
        )

    def forward(j, d):
        return remote(
            low_piece(j, d, c), low_piece(j, d, c), pf_send.at[j, d], pf_recv.at[j, d], f, t ^ 1
        )

    for j in range(2):
        total = half_own[j, at(z * chunk, chunk), :]
        for d in range(1, depth):
            z_copy(j, d).wait_recv()
            total = total + z_recv[d, j].astype(F32)
        low[j, at(c * half + z * chunk, chunk), :] = total.astype(BF)
        for d in range(1, depth):
            g_copy(j, d).start()
        forward(j, 0).start()

    def block_copy(j, o, side, target):
        piece = basis.at[j, at((2 * o + c) * columns, columns)]
        return remote(
            piece, piece, g_send.at[side, o, j], g_recv.at[o, j], f, target * 2 + c
        )

    def block_forward(j, o):
        piece = basis.at[j, at((2 * o + c) * columns, columns)]
        return remote(piece, piece, gp_send.at[o, j], gp_recv.at[o, j], f, t ^ 1)

    def needed(o):
        return f != (2 * o) // group

    def spread(j, o, side):
        if side == 0:

            @pl.when(z >= 1)
            def _():
                block_copy(j, o, 0, z - 1).start()
        else:

            @pl.when(z <= depth - 2)
            def _():
                block_copy(j, o, 1, z + 1).start()

    @pl.when(needed(z))
    def _():
        for j in range(2):
            for side in range(2):
                spread(j, z, side)

    def arrive(s):
        for side in range(2):
            o = z + s if side == 0 else z - s
            inside = o <= depth - 1 if side == 0 else o >= 0

            @pl.when(inside & needed(o))
            def _(o=o, side=side):
                for j in range(2):
                    block_copy(j, o, side, z).wait_recv()
                    spread(j, o, side)
                    block_forward(j, o).start()

    loads[5].wait()
    loads[6].wait()

    def reduce_copy(m, j):
        return remote(
            proj_send.at[j, at((f ^ m) * part, part)],
            proj_recv.at[m, j],
            rs_send.at[m, j],
            rs_recv.at[m, j],
            f ^ m,
            t,
        )

    for j in range(2):
        for d in range(1, depth):
            g_copy(j, d).wait_recv()
            forward(j, d).start()
        for d in range(depth):
            forward(j, d).wait_recv()
        product = lax.dot_general(
            low[j], cot[j], (((0,), (0,)), ((), ())), preferred_element_type=F32
        )
        proj[j] = product
        proj_send[j] = product.astype(BF)
        for m in range(1, fs):
            reduce_copy(m, j).start()
        if relay:
            share(marks[j], marks[j + 1])

    for i in range(7, 11):
        loads[i].wait()
    own = at(f * part, part)

    def ratio_copy(m, j):
        piece = ratio.at[j, own]
        return remote(piece, piece, ag_send.at[m, j], ag_recv.at[m, j], f ^ m, t)

    for j in range(2):
        for m in range(1, fs):
            reduce_copy(m, j).wait_recv()
        summed = proj[j, own, :]
        for m in range(1, fs):
            summed = summed + proj_recv[m, j].astype(F32)
        first = moment_decay * moment[2 * j] + (1.0 - moment_decay) * summed
        second = square_decay * moment[2 * j + 1] + (1.0 - square_decay) * summed * summed
        first_new[j] = first
        second_new[j] = second
        ratio[j, own, :] = (first / jnp.sqrt(second + square_floor)).astype(BF)
        for m in range(1, fs):
            ratio_copy(m, j).start()
        if relay:
            share(marks[j + 2], marks[j + 3])

    arrive(1)

    high = min(rows, 256)
    for j in range(2):
        for m in range(1, fs):
            ratio_copy(m, j).wait_recv()

        def add(i, total, j=j):
            update = jnp.dot(
                basis[j, at(f * rows + i * high, high), :], ratio[j], preferred_element_type=F32
            )
            step_ref[j, at(i * high, high), :] = update
            return total + jnp.sum((update * update).reshape(high // 8, 8, width), axis=0)

        sums[f, j] = lax.fori_loop(0, rows // high, add, jnp.zeros((8, width), F32))

    def sums_copy(m):
        return remote(sums.at[f], sums.at[f], s_send.at[m], s_recv.at[m], f ^ m, t)

    for m in range(1, fs):
        sums_copy(m).start()
    if relay:
        share(marks[4], count)
    for s in range(2, depth):
        arrive(s)
    for m in range(1, fs):
        sums_copy(m).wait_recv()
    for j in range(2):
        squares = sums[0, j]
        for k in range(1, fs):
            squares = squares + sums[k, j]
        squares = jnp.sum(squares, axis=0, keepdims=True)
        for h in range(width // HD):
            head = slice(h * HD, (h + 1) * HD)
            total = jnp.sum(squares[:, head], axis=1, keepdims=True)
            scale = 1.0 / jnp.sqrt(total / (fs * rows * HD) + norm_floor)
            scales[j, :, head] = jnp.broadcast_to(scale, (8, HD))

    def finish(j, place, update):
        step = update * scales[j, 0:1, :]
        copy_ref[j, place, :] = (gathered[j, place, :].astype(F32) - step_rate * step).astype(BF)
        return step

    for j in range(2):

        @pl.loop(0, rows // high)
        def _(i, j=j):
            place = at(i * high, high)
            step = finish(j, at(f * rows + i * high, high), step_ref[j, place, :])
            step_ref[j, place, :] = step
            weight_ref[j, place, :] = master[j, place, :] - step_rate * step

    for j in range(2):

        @pl.when(role != 0)
        def _(j=j):
            partner_copy(j).wait_recv()

    for s in range(1, depth):
        for o, inside in ((z + s, z + s <= depth - 1), (z - s, z - s >= 0)):

            @pl.when(inside & needed(o))
            def _(o=o):
                for j in range(2):
                    block_forward(j, o).wait_recv()

    def finish_rows(j, start):
        place = at(start, high)
        update = jnp.dot(basis[j, place, :], ratio[j], preferred_element_type=F32)
        finish(j, place, update)

    span = high // tile

    def finish_block(m, j, wait):
        @pl.loop(0, rows // high)
        def _(i):
            if wait is not None:
                for k in range(span):
                    wait(i * span + k)
            finish_rows(j, (f ^ m) * rows + i * high)

    if relay:
        finish_block(1, 0, None)
        finish_block(2, 1, None)
        finish_block(1, 1, lambda i: master_copy(1, 1, i).wait_recv())
        finish_block(2, 0, lambda i: master_copy(2, 0, i).wait_recv())

        @pl.loop(0, rows // high)
        def _(i):
            for m in (2, 1):
                for k in range(span):
                    relay_copy(m, i * span + k).wait_recv()
                finish_rows(2 - m, (f ^ 3) * rows + i * high)
    else:
        for m in range(1, fs):
            for j in range(2):
                finish_block(m, j, lambda i, m=m, j=j: master_copy(m, j, i).wait_recv())

    if relay:

        @pl.when(role != 2)
        def _():
            for j in range(2):
                basis_copy(0, j, 0, f).wait_send()

        @pl.when(role != 1)
        def _():
            for j in range(2):
                basis_copy(0, j, 1, f).wait_send()
    else:

        @pl.when(role == 0)
        def _():
            for m in range(1, fs):
                for j in range(2):
                    for h in range(2):
                        basis_copy(m, j, h, f ^ m).wait_send()

    for j in range(2):

        @pl.when(role != 0)
        def _(j=j):
            partner_copy(j).wait_send()

        swap(j).wait_send()
        for d in range(1, depth):
            z_copy(j, d).wait_send()
            g_copy(j, d).wait_send()
        for d in range(depth):
            forward(j, d).wait_send()
        for m in range(1, fs):
            reduce_copy(m, j).wait_send()
            ratio_copy(m, j).wait_send()
    for m in range(1, fs):
        sums_copy(m).wait_send()

    for s in range(depth):
        for side in range(2):
            o = z + s if side == 0 else z - s
            inside = (o <= depth - 1) & (z >= 1) if side == 0 else (o >= 0) & (z <= depth - 2)

            @pl.when(inside & needed(o))
            def _(o=o, side=side):
                for j in range(2):
                    block_copy(j, o, side, z).wait_send()

            if s > 0:
                there = o <= depth - 1 if side == 0 else o >= 0

                @pl.when(there & needed(o))
                def _(o=o):
                    for j in range(2):
                        block_forward(j, o).wait_send()

    for m in (1, 2) if relay else range(1, fs):
        piece = gathered.at[:, own_rows]
        remote(piece, piece, m_send.at[m - 1], m_recv.at[m - 1, 0, 0], f ^ m, t).wait_send()
    if relay:
        for m in (1, 2):
            piece = gathered.at[2 - m, own_rows]
            remote(piece, piece, r_send.at[m - 1], r_recv.at[m - 1, 0], f ^ m, t).wait_send()


MARKS = (13, 14, 15, 16, 18)
FIRST = ((8, 8), (4, 1), (1, 4), (3, 3))


def final_kernel(*refs):
    first, second, step, weight, copy = refs[:5]
    outs, sem = refs[5:15], refs[15]
    moves = []
    for j in range(2):
        for k, source in enumerate((step, weight, copy, first, second)):
            moves.append((source.at[j], outs[5 * j + k]))
    moves = [pltpu.make_async_copy(a, b, sem.at[i]) for i, (a, b) in enumerate(moves)]
    for move in moves:
        move.start()
    for move in moves:
        move.wait()


def body(fs, tp, *args):
    saved_input, query_cot, _, query_master, key_master, query_basis, key_basis = args[:7]
    rows, rank = query_basis.shape
    tokens, columns = saved_input.shape
    width = query_cot.shape[1]
    part = rank // fs
    depth = tp // 2
    count = fs * rows
    half, chunk = tokens // 2, tokens // tp
    pieces = rows // min(rows, 128)
    hbm = pl.BlockSpec(memory_space=pltpu.HBM)
    vmem = pl.BlockSpec(memory_space=pltpu.VMEM)
    dma = pltpu.SemaphoreType.DMA
    own = pltpu.VMEM((2, rows, width), F32)
    moment = pltpu.VMEM((2, part, width), F32)
    pairs = [dma((fs, 2, 2)), dma((2, 2))]
    for shape in (
        (2,),
        (2,),
        (2, depth),
        (2, depth),
        (2, depth),
    ):
        pairs += [dma(shape), dma(shape)]
    pairs += [dma((2, depth, 2)), dma((depth, 2))]
    for shape in ((depth, 2), (fs, 2), (fs, 2), (fs,)):
        pairs += [dma(shape), dma(shape)]
    links = 2 if fs == 4 else fs - 1
    pairs += [dma((links,)), dma((links, 2, pieces)), dma((2,)), dma((2, pieces))]
    results = pl.pallas_call(
        functools.partial(exchange_kernel, fs, tp),
        name="exchange",
        out_shape=(moment, moment, own, own, pltpu.VMEM((2, count, width), BF)),
        in_specs=[hbm] * 11,
        out_specs=(vmem,) * 5,
        scratch_shapes=[
            pltpu.VMEM((2, count, rank), BF),
            pltpu.VMEM((2, count, width), BF),
            pltpu.VMEM((tokens, columns), BF),
            pltpu.VMEM((2, tokens, width), BF),
            pltpu.VMEM((2, rows, width), F32),
            pltpu.VMEM((4, part, width), F32),
            pltpu.VMEM((2, half, rank), BF),
            pltpu.VMEM((2, half, rank), BF),
            pltpu.VMEM((2, half, rank), F32),
            pltpu.VMEM((2, half, rank), BF),
            pltpu.VMEM((depth, 2, chunk, rank), BF),
            pltpu.VMEM((2, tokens, rank), BF),
            pltpu.VMEM((2, rank, width), F32),
            pltpu.VMEM((2, rank, width), BF),
            pltpu.VMEM((fs, 2, part, width), BF),
            pltpu.VMEM((2, rank, width), BF),
            pltpu.VMEM((fs, 2, 8, width), F32),
            pltpu.VMEM((2, 8, width), F32),
            dma((11,)),
            *pairs,
        ],
        compiler_params=pltpu.CompilerParams(
            collective_id=0, has_side_effects=True, vmem_limit_bytes=40 * 1024 * 1024
        ),
    )(*[pltpu.with_memory_space_constraint(a, pltpu.HBM) for a in args])

    big = jax.ShapeDtypeStruct((rows, width), F32)
    copied = jax.ShapeDtypeStruct((count, width), BF)
    small = jax.ShapeDtypeStruct((part, width), F32)
    return pl.pallas_call(
        final_kernel,
        name="final",
        out_shape=(big, big, copied, small, small) * 2,
        in_specs=[vmem] * 5,
        out_specs=(hbm,) * 10,
        scratch_shapes=[dma((10,))],
        compiler_params=pltpu.CompilerParams(vmem_limit_bytes=20 * 1024 * 1024),
    )(*results)


def solution(mesh):
    split, tall, wide = P("fs", "tp"), P("fs", None), P(None, "tp")
    outs = (split, split, wide, split, split)
    return jax.shard_map(
        functools.partial(body, mesh.shape["fs"], mesh.shape["tp"]),
        mesh=mesh,
        in_specs=(split,) * 5 + (tall, tall) + (split,) * 4,
        out_specs=outs + outs,
        check_vma=False,
    )
```

time: 122 us -> 102 us (0.84); the launches traced: 122 us -> 99.6 us
  Pallas kernels: 121 us -> 98.9 us
    pallas_call x1, Pallas kernels: 106 us -> 92.8 us  [body(): pl.pallas_call(functools.partial(exchange_kernel, fs, tp), name='exchange...]
    pallas_call x1, Pallas kernels: 15.6 us -> 6.09 us  [body(): pl.pallas_call(final_kernel, name='final', out_shape=(big, big, copied, s...]
where the time goes in v1:
time: 102 us; the launch traced here: 99.6 us
  Pallas kernels  98.9 us (97%)
    pallas_call x1, Pallas kernels, body(): pl.pallas_call(functools.partial(exchange_kernel, fs, tp), name='exchange...  92.8 us
    pallas_call x1, Pallas kernels, body(): pl.pallas_call(final_kernel, name='final', out_shape=(big, big, copied, s...  6.09 us

profile of v1, /device:TPU:0, one launch (start us, length us, event | category | flops | bytes accessed | tf_op | source)
XLA Modules:
  0.0 99.6 jit_solution(541884220718991924)
XLA Ops:
  0.6 92.8 %exchange.1 = (f32[2,64,512]{2,1,0:T(8,128)S(1)}, f32[2,64,512]{2,1,0:T(8,128)S(1)}, f32[2,1024,512]{2,1,0:T(8,128)S(1)}, f32[2,1024,512]{2,1,0:T(8,128)S(1)}, bf16[2,4096,512]{2,1,0:T(8,128)(2,1)S(1)}) custom-call(bf16[1024,512]{1,0:T(8,128)(2,1)} %x_hbm.1, bf16[1024,512]{1,0:T(8,128)(2,1)} %qc_hbm.1, bf16[1024,512]{1,0:T(8,128)(2,1)} %kc_hbm.1, ...), custom_call_target="tpu_custom_call" | custom-call | tf_op jit(solution)/shard_map/exchange/pallas_call | solution.py:665
  93.5 6.1 %final.1 = (f32[1024,512]{1,0:T(8,128)}, f32[1024,512]{1,0:T(8,128)}, bf16[4096,512]{1,0:T(8,128)(2,1)}, f32[64,512]{1,0:T(8,128)}, f32[64,512]{1,0:T(8,128)}, /...) custom-call(f32[2,64,512]{2,1,0:T(8,128)S(1)} %get-tuple-element.15., ...), custom_call_target="tpu_custom_call" | custom-call | tf_op jit(solution)/shard_map/final/pallas_call | solution.py:701

commit v2 on v1

--- a/solution.py
+++ b/solution.py
@@ -54,6 +54,7 @@
     proj,
     proj_send,
     proj_recv,
+    proj_mid,
     ratio,
     sums,
     scales,
@@ -181,7 +182,7 @@
 
     def basis_copy(m, j, h, target):
         piece = basis.at[j, at(t * columns + h * piece_rows, piece_rows)]
-        return remote(piece, piece, b_send.at[m, j, h], b_recv.at[j, h], target, t)
+        return remote(piece, piece, b_send.at[0], b_recv.at[j, h], target, t)
 
     loads[0].wait()
     loads[1].wait()
@@ -272,7 +273,7 @@
 
     def partner_copy(j):
         piece = basis.at[j, at(t * columns, columns)]
-        return remote(piece, piece, d_send.at[j], d_recv.at[j], f, t ^ 1)
+        return remote(piece, piece, d_send.at[0], d_recv.at[0], f, t ^ 1)
 
     step = min(half, 256)
 
@@ -284,15 +285,15 @@
         )
 
     def swap(j):
-        return remote(half_send.at[j], half_recv.at[j], p_send.at[j], p_recv.at[j], f, t ^ 1)
+        return remote(half_send.at[j], half_recv.at[j], p_send.at[0], p_recv.at[j], f, t ^ 1)
 
     def z_copy(j, d):
         other = lax.rem(z + d, depth)
         return remote(
             z_send.at[j, at(other * chunk, chunk)],
-            z_recv.at[d, j],
-            zr_send.at[j, d],
-            zr_recv.at[j, d],
+            z_recv.at[j, d],
+            zr_send.at[0],
+            zr_recv.at[j],
             f,
             other * 2 + c,
         )
@@ -335,22 +336,23 @@
         return remote(
             low_piece(j, 0, c),
             low_piece(j, 0, c),
-            zg_send.at[j, d],
-            zg_recv.at[j, d],
+            zg_send.at[0],
+            zg_recv.at[j, d - 1],
             f,
             other * 2 + c,
         )
 
     def forward(j, d):
         return remote(
-            low_piece(j, d, c), low_piece(j, d, c), pf_send.at[j, d], pf_recv.at[j, d], f, t ^ 1
+            low_piece(j, d, c), low_piece(j, d, c), pf_send.at[0], pf_recv.at[j], f, t ^ 1
         )
 
     for j in range(2):
         total = half_own[j, at(z * chunk, chunk), :]
+        received = z_recv.at[j, 1:depth]
+        remote(received, received, zr_send.at[0], zr_recv.at[j], f, t ^ 1).wait_recv()
         for d in range(1, depth):
-            z_copy(j, d).wait_recv()
-            total = total + z_recv[d, j].astype(F32)
+            total = total + z_recv[j, d].astype(F32)
         low[j, at(c * half + z * chunk, chunk), :] = total.astype(BF)
         for d in range(1, depth):
             g_copy(j, d).start()
@@ -359,12 +361,12 @@
     def block_copy(j, o, side, target):
         piece = basis.at[j, at((2 * o + c) * columns, columns)]
         return remote(
-            piece, piece, g_send.at[side, o, j], g_recv.at[o, j], f, target * 2 + c
+            piece, piece, g_send.at[side, o], g_recv.at[o, j], f, target * 2 + c
         )
 
     def block_forward(j, o):
         piece = basis.at[j, at((2 * o + c) * columns, columns)]
-        return remote(piece, piece, gp_send.at[o, j], gp_recv.at[o, j], f, t ^ 1)
+        return remote(piece, piece, gp_send.at[o], gp_recv.at[o], f, t ^ 1)
 
     def needed(o):
         return f != (2 * o) // group
@@ -402,62 +404,93 @@
     loads[5].wait()
     loads[6].wait()
 
-    def reduce_copy(m, j):
-        return remote(
-            proj_send.at[j, at((f ^ m) * part, part)],
-            proj_recv.at[m, j],
-            rs_send.at[m, j],
-            rs_recv.at[m, j],
-            f ^ m,
-            t,
-        )
-
-    for j in range(2):
+    own = at(f * part, part)
+
+    def project_low(j):
         for d in range(1, depth):
             g_copy(j, d).wait_recv()
             forward(j, d).start()
-        for d in range(depth):
-            forward(j, d).wait_recv()
+        received = low.at[j, at((1 - c) * half, half)]
+        remote(received, received, pf_send.at[0], pf_recv.at[j], f, t ^ 1).wait_recv()
         product = lax.dot_general(
             low[j], cot[j], (((0,), (0,)), ((), ())), preferred_element_type=F32
         )
         proj[j] = product
         proj_send[j] = product.astype(BF)
-        for m in range(1, fs):
-            reduce_copy(m, j).start()
-        if relay:
-            share(marks[j], marks[j + 1])
-
-    for i in range(7, 11):
-        loads[i].wait()
-    own = at(f * part, part)
-
-    def ratio_copy(m, j):
-        piece = ratio.at[j, own]
-        return remote(piece, piece, ag_send.at[m, j], ag_recv.at[m, j], f ^ m, t)
-
-    for j in range(2):
-        for m in range(1, fs):
-            reduce_copy(m, j).wait_recv()
-        summed = proj[j, own, :]
-        for m in range(1, fs):
-            summed = summed + proj_recv[m, j].astype(F32)
+
+    def update_moments(j, summed):
         first = moment_decay * moment[2 * j] + (1.0 - moment_decay) * summed
         second = square_decay * moment[2 * j + 1] + (1.0 - square_decay) * summed * summed
         first_new[j] = first
         second_new[j] = second
         ratio[j, own, :] = (first / jnp.sqrt(second + square_floor)).astype(BF)
-        for m in range(1, fs):
-            ratio_copy(m, j).start()
+
+    def reduce_copy(j, k):
+        near, far = (1, 2) if j == 0 else (2, 1)
         if relay:
-            share(marks[j + 2], marks[j + 3])
-
+            source = proj_mid.at[j] if k == 3 else proj_send.at[j, at((f ^ (near, 3)[k - 1]) * part, part)]
+            target = f ^ (far if k == 3 else near)
+        else:
+            source, target = proj_send.at[j, at((f ^ k) * part, part)], f ^ k
+        return remote(
+            source, proj_recv.at[j, k], rs_send.at[0], rs_recv.at[j, k - 1], target, t
+        )
+
+    def ratio_copy(j, k):
+        near, far = (1, 2) if j == 0 else (2, 1)
+        if relay:
+            piece = ratio.at[j, at((f ^ near) * part, part) if k == 3 else own]
+            target = f ^ (near if k == 1 else far)
+        else:
+            piece, target = ratio.at[j, own], f ^ k
+        return remote(piece, piece, ag_send.at[0], ag_recv.at[j, k - 1], target, t)
+
+    for j in range(2):
+        project_low(j)
+        for k in (2, 1) if relay else range(1, fs):
+            reduce_copy(j, k).start()
+        if relay:
+            share(marks[j], marks[j + 1])
+
+    if relay:
+        for j in range(2):
+            far = 2 if j == 0 else 1
+            reduce_copy(j, 2).wait_recv()
+            mid = proj[j, at((f ^ far) * part, part), :] + proj_recv[j, 2].astype(F32)
+            proj_mid[j] = mid.astype(BF)
+            reduce_copy(j, 3).start()
+        share(marks[2], marks[3])
     arrive(1)
+    for i in range(7, 11):
+        loads[i].wait()
+
+    for j in range(2):
+        summed = proj[j, own, :]
+        for k in (1, 3) if relay else range(1, fs):
+            reduce_copy(j, k).wait_recv()
+            summed = summed + proj_recv[j, k].astype(F32)
+        update_moments(j, summed)
+        for k in (1, 2) if relay else range(1, fs):
+            ratio_copy(j, k).start()
+    if relay:
+        share(marks[3], marks[4])
+        for j in range(2):
+            ratio_copy(j, 1).wait_recv()
+            ratio_copy(j, 3).start()
+        share(marks[4], marks[5])
+
+    def ratio_wait(j):
+        for k in (2, 3) if relay else range(1, fs):
+            ratio_copy(j, k).wait_recv()
+
+    if depth > 2:
+        arrive(2)
 
     high = min(rows, 256)
-    for j in range(2):
-        for m in range(1, fs):
-            ratio_copy(m, j).wait_recv()
+    heads = width // HD
+    sums[f] = jnp.zeros(sums.shape[1:], F32)
+    for j in range(2):
+        ratio_wait(j)
 
         def add(i, total, j=j):
             update = jnp.dot(
@@ -466,57 +499,64 @@
             step_ref[j, at(i * high, high), :] = update
             return total + jnp.sum((update * update).reshape(high // 8, 8, width), axis=0)
 
-        sums[f, j] = lax.fori_loop(0, rows // high, add, jnp.zeros((8, width), F32))
+        squares = lax.fori_loop(0, rows // high, add, jnp.zeros((8, width), F32))
+        for h in range(heads):
+            total = jnp.sum(squares[:, h * HD : (h + 1) * HD])
+            sums[f, j * heads + h : j * heads + h + 1, :] = jnp.broadcast_to(total, (1, HD))
 
     def sums_copy(m):
-        return remote(sums.at[f], sums.at[f], s_send.at[m], s_recv.at[m], f ^ m, t)
+        return remote(sums.at[f], sums.at[f], s_send.at[0], s_recv.at[0], f ^ m, t)
 
     for m in range(1, fs):
         sums_copy(m).start()
     if relay:
-        share(marks[4], count)
-    for s in range(2, depth):
+        share(marks[5], count)
+    for s in range(3, depth):
         arrive(s)
-    for m in range(1, fs):
-        sums_copy(m).wait_recv()
-    for j in range(2):
-        squares = sums[0, j]
-        for k in range(1, fs):
-            squares = squares + sums[k, j]
-        squares = jnp.sum(squares, axis=0, keepdims=True)
-        for h in range(width // HD):
-            head = slice(h * HD, (h + 1) * HD)
-            total = jnp.sum(squares[:, head], axis=1, keepdims=True)
-            scale = 1.0 / jnp.sqrt(total / (fs * rows * HD) + norm_floor)
-            scales[j, :, head] = jnp.broadcast_to(scale, (8, HD))
+    others = sums.at[0 : fs - 1]
+    remote(others, others, s_send.at[0], s_recv.at[0], f ^ 1, t).wait_recv()
+    total = sums[0]
+    for k in range(1, fs):
+        total = total + sums[k]
+    factor = 1.0 / jnp.sqrt(total / (fs * rows * HD) + norm_floor)
+    for j in range(2):
+        for h in range(heads):
+            row = factor[j * heads + h : j * heads + h + 1, :]
+            scales[j, :, h * HD : (h + 1) * HD] = jnp.broadcast_to(row, (8, HD))
 
     def finish(j, place, update):
-        step = update * scales[j, 0:1, :]
-        copy_ref[j, place, :] = (gathered[j, place, :].astype(F32) - step_rate * step).astype(BF)
-        return step
+        change = update * (step_rate * scales[j, 0:1, :])
+        copy_ref[j, place, :] = (gathered[j, place, :].astype(F32) - change).astype(BF)
 
     for j in range(2):
 
         @pl.loop(0, rows // high)
         def _(i, j=j):
             place = at(i * high, high)
-            step = finish(j, at(f * rows + i * high, high), step_ref[j, place, :])
+            update = step_ref[j, place, :]
+            finish(j, at(f * rows + i * high, high), update)
+            step = update * scales[j, 0:1, :]
             step_ref[j, place, :] = step
             weight_ref[j, place, :] = master[j, place, :] - step_rate * step
 
-    for j in range(2):
-
-        @pl.when(role != 0)
-        def _(j=j):
-            partner_copy(j).wait_recv()
+    def both(o, core):
+        return basis.at[:, at((2 * o + core) * columns, columns)]
+
+    def partner_block():
+        piece = both(z, 1 - c)
+        return remote(piece, piece, d_send.at[0], d_recv.at[0], f, t ^ 1)
+
+    @pl.when(role != 0)
+    def _():
+        partner_block().wait_recv()
 
     for s in range(1, depth):
         for o, inside in ((z + s, z + s <= depth - 1), (z - s, z - s >= 0)):
 
             @pl.when(inside & needed(o))
             def _(o=o):
-                for j in range(2):
-                    block_forward(j, o).wait_recv()
+                piece = both(o, 1 - c)
+                remote(piece, piece, gp_send.at[o], gp_recv.at[o], f, t ^ 1).wait_recv()
 
     def finish_rows(j, start):
         place = at(start, high)
@@ -550,61 +590,49 @@
             for j in range(2):
                 finish_block(m, j, lambda i, m=m, j=j: master_copy(m, j, i).wait_recv())
 
+    def sent(piece, sem):
+        remote(piece, piece, sem, p_recv.at[0], f, t ^ 1).wait_send()
+
     if relay:
-
-        @pl.when(role != 2)
-        def _():
-            for j in range(2):
-                basis_copy(0, j, 0, f).wait_send()
-
-        @pl.when(role != 1)
-        def _():
-            for j in range(2):
-                basis_copy(0, j, 1, f).wait_send()
+        for k in range(4):
+
+            @pl.when(role == k)
+            def _(k=k):
+                sent(basis.at[:, 0 : columns if k in (0, 3) else piece_rows], b_send.at[0])
     else:
 
         @pl.when(role == 0)
         def _():
             for m in range(1, fs):
-                for j in range(2):
-                    for h in range(2):
-                        basis_copy(m, j, h, f ^ m).wait_send()
-
-    for j in range(2):
-
-        @pl.when(role != 0)
-        def _(j=j):
-            partner_copy(j).wait_send()
-
-        swap(j).wait_send()
-        for d in range(1, depth):
-            z_copy(j, d).wait_send()
-            g_copy(j, d).wait_send()
-        for d in range(depth):
-            forward(j, d).wait_send()
-        for m in range(1, fs):
-            reduce_copy(m, j).wait_send()
-            ratio_copy(m, j).wait_send()
-    for m in range(1, fs):
-        sums_copy(m).wait_send()
+                sent(basis.at[:, 0:columns], b_send.at[0])
+
+    @pl.when(role != 0)
+    def _():
+        sent(both(z, c), d_send.at[0])
+
+    sent(half_send, p_send.at[0])
+    sent(z_send.at[:, 0 : (depth - 1) * chunk], zr_send.at[0])
+    sent(low.at[:, 0 : (depth - 1) * chunk], zg_send.at[0])
+    sent(low.at[:, 0 : depth * chunk], pf_send.at[0])
+    sent(proj_send.at[:, 0 : (fs - 1) * part], rs_send.at[0])
+    sent(ratio.at[:, 0 : (fs - 1) * part], ag_send.at[0])
+    sent(others, s_send.at[0])
 
     for s in range(depth):
         for side in range(2):
             o = z + s if side == 0 else z - s
-            inside = (o <= depth - 1) & (z >= 1) if side == 0 else (o >= 0) & (z <= depth - 2)
+            there = o <= depth - 1 if side == 0 else o >= 0
+            inside = there & (z >= 1) if side == 0 else there & (z <= depth - 2)
 
             @pl.when(inside & needed(o))
             def _(o=o, side=side):
-                for j in range(2):
-                    block_copy(j, o, side, z).wait_send()
+                sent(both(o, c), g_send.at[side, o])
 
             if s > 0:
-                there = o <= depth - 1 if side == 0 else o >= 0
 
                 @pl.when(there & needed(o))
                 def _(o=o):
-                    for j in range(2):
-                        block_forward(j, o).wait_send()
+                    sent(both(o, c), gp_send.at[o])
 
     for m in (1, 2) if relay else range(1, fs):
         piece = gathered.at[:, own_rows]
@@ -615,7 +643,7 @@
             remote(piece, piece, r_send.at[m - 1], r_recv.at[m - 1, 0], f ^ m, t).wait_send()
 
 
-MARKS = (13, 14, 15, 16, 18)
+MARKS = (13, 13, 14, 15, 16, 18)
 FIRST = ((8, 8), (4, 1), (1, 4), (3, 3))
 
 
@@ -648,18 +676,19 @@
     dma = pltpu.SemaphoreType.DMA
     own = pltpu.VMEM((2, rows, width), F32)
     moment = pltpu.VMEM((2, part, width), F32)
-    pairs = [dma((fs, 2, 2)), dma((2, 2))]
-    for shape in (
-        (2,),
-        (2,),
-        (2, depth),
-        (2, depth),
-        (2, depth),
-    ):
-        pairs += [dma(shape), dma(shape)]
-    pairs += [dma((2, depth, 2)), dma((depth, 2))]
-    for shape in ((depth, 2), (fs, 2), (fs, 2), (fs,)):
-        pairs += [dma(shape), dma(shape)]
+    pairs = [
+        *(dma((1,)), dma((2, 2))),
+        *(dma((1,)), dma((1,))),
+        *(dma((1,)), dma((2,))),
+        *(dma((1,)), dma((2,))),
+        *(dma((1,)), dma((2, depth - 1))),
+        *(dma((1,)), dma((2,))),
+        *(dma((2, depth)), dma((depth, 2))),
+        *(dma((depth,)), dma((depth,))),
+        *(dma((1,)), dma((2, fs - 1))),
+        *(dma((1,)), dma((2, fs - 1))),
+        *(dma((1,)), dma((1,))),
+    ]
     links = 2 if fs == 4 else fs - 1
     pairs += [dma((links,)), dma((links, 2, pieces)), dma((2,)), dma((2, pieces))]
     results = pl.pallas_call(
@@ -679,13 +708,14 @@
             pltpu.VMEM((2, half, rank), BF),
             pltpu.VMEM((2, half, rank), F32),
             pltpu.VMEM((2, half, rank), BF),
-            pltpu.VMEM((depth, 2, chunk, rank), BF),
+            pltpu.VMEM((2, depth, chunk, rank), BF),
             pltpu.VMEM((2, tokens, rank), BF),
             pltpu.VMEM((2, rank, width), F32),
             pltpu.VMEM((2, rank, width), BF),
-            pltpu.VMEM((fs, 2, part, width), BF),
+            pltpu.VMEM((2, fs, part, width), BF),
+            pltpu.VMEM((2, part, width), BF),
             pltpu.VMEM((2, rank, width), BF),
-            pltpu.VMEM((fs, 2, 8, width), F32),
+            pltpu.VMEM((fs, -(-2 * width // HD // 8) * 8, HD), F32),
             pltpu.VMEM((2, 8, width), F32),
             dma((11,)),
             *pairs,

time: 102 us -> 96.6 us (0.947); the launches traced: 99.6 us -> 96.4 us
  Pallas kernels: 98.9 us -> 95.7 us
    pallas_call x1, Pallas kernels: 92.8 us -> 89.7 us  [body(): pl.pallas_call(functools.partial(exchange_kernel, fs, tp), name='exchange...]
where the time goes in v2:
time: 96.6 us; the launch traced here: 96.4 us
  Pallas kernels  95.7 us (99%)
    pallas_call x1, Pallas kernels, body(): pl.pallas_call(functools.partial(exchange_kernel, fs, tp), name='exchange...  89.7 us
    pallas_call x1, Pallas kernels, body(): pl.pallas_call(final_kernel, name='final', out_shape=(big, big, copied, s...  6.09 us

profile of v2, /device:TPU:0, one launch (start us, length us, event | category | flops | bytes accessed | tf_op | source)
XLA Modules:
  0.0 96.4 jit_solution(7978508112913536717)
XLA Ops:
  0.6 89.7 %exchange.1 = (f32[2,64,512]{2,1,0:T(8,128)S(1)}, f32[2,64,512]{2,1,0:T(8,128)S(1)}, f32[2,1024,512]{2,1,0:T(8,128)S(1)}, f32[2,1024,512]{2,1,0:T(8,128)S(1)}, bf16[2,4096,512]{2,1,0:T(8,128)(2,1)S(1)}) custom-call(bf16[1024,512]{1,0:T(8,128)(2,1)} %x_hbm.1, bf16[1024,512]{1,0:T(8,128)(2,1)} %qc_hbm.1, bf16[1024,512]{1,0:T(8,128)(2,1)} %kc_hbm.1, ...), custom_call_target="tpu_custom_call" | custom-call | tf_op jit(solution)/shard_map/exchange/pallas_call | solution.py:694
  90.3 6.1 %final.1 = (f32[1024,512]{1,0:T(8,128)}, f32[1024,512]{1,0:T(8,128)}, bf16[4096,512]{1,0:T(8,128)(2,1)}, f32[64,512]{1,0:T(8,128)}, f32[64,512]{1,0:T(8,128)}, /...) custom-call(f32[2,64,512]{2,1,0:T(8,128)S(1)} %get-tuple-element.15., ...), custom_call_target="tpu_custom_call" | custom-call | tf_op jit(solution)/shard_map/final/pallas_call | solution.py:731

commit v3 on v2

--- a/solution.py
+++ b/solution.py
@@ -100,7 +100,7 @@
     group = rows // columns
     owner = t // group
     role = f ^ owner
-    tile = min(rows, 128)
+    tile = min(rows, 256) // 2
     pieces = rows // tile
 
     def at(start, size):
@@ -131,7 +131,7 @@
         (ks_hbm, moment.at[3]),
     )
     loads = [
-        pltpu.make_async_copy(source, target, load_sem.at[i])
+        pltpu.make_async_copy(source, target, load_sem.at[(0, 1, 2, 3, 4, 5, 5, 6, 6, 6, 6)[i]])
         for i, (source, target) in enumerate(sources)
     ]
     for load in loads:
@@ -147,11 +147,19 @@
 
     def master_copy(m, j, i):
         piece = gathered.at[j, at(f * rows + i * tile, tile)]
-        return remote(piece, piece, m_send.at[m - 1], m_recv.at[m - 1, j, i], f ^ m, t)
+        return remote(piece, piece, m_send.at[m - 1], m_recv.at[m - 1, j, i // 2], f ^ m, t)
 
     def relay_copy(m, i):
         piece = gathered.at[2 - m, at((f ^ (3 - m)) * rows + i * tile, tile)]
-        return remote(piece, piece, r_send.at[m - 1], r_recv.at[m - 1, i], f ^ m, t)
+        return remote(piece, piece, r_send.at[m - 1], r_recv.at[m - 1, i // 2], f ^ m, t)
+
+    def master_wait(m, j, i):
+        pair = gathered.at[j, at((f ^ m) * rows + i * 2 * tile, 2 * tile)]
+        remote(pair, pair, m_send.at[m - 1], m_recv.at[m - 1, j, i], f ^ m, t).wait_recv()
+
+    def relay_wait(m, i):
+        pair = gathered.at[2 - m, at((f ^ 3) * rows + i * 2 * tile, 2 * tile)]
+        remote(pair, pair, r_send.at[m - 1], r_recv.at[m - 1, i], f ^ m, t).wait_recv()
 
     def issue(m, start, stop):
         for turn in range(2):
@@ -166,10 +174,11 @@
         low_end, high_end = max(start, 2 * pieces), min(stop, 3 * pieces)
         if low_end < high_end:
 
-            @pl.loop(low_end - 2 * pieces, high_end - 2 * pieces)
+            @pl.loop(low_end // 2 - pieces, high_end // 2 - pieces)
             def _(i):
-                master_copy(3 - m, 2 - m, i).wait_recv()
-                relay_copy(m, i).start()
+                master_wait(3 - m, 2 - m, i)
+                relay_copy(m, 2 * i).start()
+                relay_copy(m, 2 * i + 1).start()
 
     def share(start, stop):
         for m in (1, 2):
@@ -177,6 +186,7 @@
 
     count = 3 * pieces
     marks = [count * k // 24 for k in MARKS]
+    marks = [k if k <= 2 * pieces else k // 2 * 2 for k in marks]
 
     piece_rows = columns // 2
 
@@ -401,8 +411,7 @@
                     spread(j, o, side)
                     block_forward(j, o).start()
 
-    loads[5].wait()
-    loads[6].wait()
+    pltpu.make_async_copy(cot, cot, load_sem.at[5]).wait()
 
     own = at(f * part, part)
 
@@ -461,8 +470,7 @@
             reduce_copy(j, 3).start()
         share(marks[2], marks[3])
     arrive(1)
-    for i in range(7, 11):
-        loads[i].wait()
+    pltpu.make_async_copy(moment, moment, load_sem.at[6]).wait()
 
     for j in range(2):
         summed = proj[j, own, :]
@@ -558,37 +566,37 @@
                 piece = both(o, 1 - c)
                 remote(piece, piece, gp_send.at[o], gp_recv.at[o], f, t ^ 1).wait_recv()
 
-    def finish_rows(j, start):
-        place = at(start, high)
+    def finish_rows(j, start, size):
+        place = at(start, size)
         update = jnp.dot(basis[j, place, :], ratio[j], preferred_element_type=F32)
         finish(j, place, update)
 
-    span = high // tile
+    large = min(rows, 512)
+    pair = 2 * tile
 
     def finish_block(m, j, wait):
-        @pl.loop(0, rows // high)
+        @pl.loop(0, rows // large)
         def _(i):
-            if wait is not None:
-                for k in range(span):
-                    wait(i * span + k)
-            finish_rows(j, (f ^ m) * rows + i * high)
+            if wait:
+                for k in range(large // pair):
+                    master_wait(m, j, i * (large // pair) + k)
+            finish_rows(j, (f ^ m) * rows + i * large, large)
 
     if relay:
-        finish_block(1, 0, None)
-        finish_block(2, 1, None)
-        finish_block(1, 1, lambda i: master_copy(1, 1, i).wait_recv())
-        finish_block(2, 0, lambda i: master_copy(2, 0, i).wait_recv())
-
-        @pl.loop(0, rows // high)
+        finish_block(1, 0, False)
+        finish_block(2, 1, False)
+        finish_block(1, 1, True)
+        finish_block(2, 0, True)
+
+        @pl.loop(0, rows // pair)
         def _(i):
             for m in (2, 1):
-                for k in range(span):
-                    relay_copy(m, i * span + k).wait_recv()
-                finish_rows(2 - m, (f ^ 3) * rows + i * high)
+                relay_wait(m, i)
+                finish_rows(2 - m, (f ^ 3) * rows + i * pair, pair)
     else:
         for m in range(1, fs):
             for j in range(2):
-                finish_block(m, j, lambda i, m=m, j=j: master_copy(m, j, i).wait_recv())
+                finish_block(m, j, True)
 
     def sent(piece, sem):
         remote(piece, piece, sem, p_recv.at[0], f, t ^ 1).wait_send()
@@ -643,8 +651,8 @@
             remote(piece, piece, r_send.at[m - 1], r_recv.at[m - 1, 0], f ^ m, t).wait_send()
 
 
-MARKS = (13, 13, 14, 15, 16, 18)
-FIRST = ((8, 8), (4, 1), (1, 4), (3, 3))
+MARKS = (14, 14, 15, 16, 18, 20)
+FIRST = ((8, 8), (5, 2), (2, 5), (4, 4))
 
 
 def final_kernel(*refs):
@@ -670,7 +678,7 @@
     depth = tp // 2
     count = fs * rows
     half, chunk = tokens // 2, tokens // tp
-    pieces = rows // min(rows, 128)
+    pieces = rows // (min(rows, 256) // 2)
     hbm = pl.BlockSpec(memory_space=pltpu.HBM)
     vmem = pl.BlockSpec(memory_space=pltpu.VMEM)
     dma = pltpu.SemaphoreType.DMA
@@ -690,7 +698,7 @@
         *(dma((1,)), dma((1,))),
     ]
     links = 2 if fs == 4 else fs - 1
-    pairs += [dma((links,)), dma((links, 2, pieces)), dma((2,)), dma((2, pieces))]
+    pairs += [dma((links,)), dma((links, 2, pieces // 2)), dma((2,)), dma((2, pieces // 2))]
     results = pl.pallas_call(
         functools.partial(exchange_kernel, fs, tp),
         name="exchange",
@@ -717,7 +725,7 @@
             pltpu.VMEM((2, rank, width), BF),
             pltpu.VMEM((fs, -(-2 * width // HD // 8) * 8, HD), F32),
             pltpu.VMEM((2, 8, width), F32),
-            dma((11,)),
+            dma((7,)),
             *pairs,
         ],
         compiler_params=pltpu.CompilerParams(

time: 96.6 us -> 95.9 us (level)
  no operation moved by 1% of the time
where the time goes in v3:
time: 95.9 us; the launch traced here: 95.6 us
  Pallas kernels  95 us (99%)
    pallas_call x1, Pallas kernels, body(): pl.pallas_call(functools.partial(exchange_kernel, fs, tp), name='exchange...  88.9 us
    pallas_call x1, Pallas kernels, body(): pl.pallas_call(final_kernel, name='final', out_shape=(big, big, copied, s...  6.09 us

profile of v3, /device:TPU:0, one launch (start us, length us, event | category | flops | bytes accessed | tf_op | source)
XLA Modules:
  0.0 95.6 jit_solution(5527570919199576946)
XLA Ops:
  0.6 88.9 %exchange.1 = (f32[2,64,512]{2,1,0:T(8,128)S(1)}, f32[2,64,512]{2,1,0:T(8,128)S(1)}, f32[2,1024,512]{2,1,0:T(8,128)S(1)}, f32[2,1024,512]{2,1,0:T(8,128)S(1)}, bf16[2,4096,512]{2,1,0:T(8,128)(2,1)S(1)}) custom-call(bf16[1024,512]{1,0:T(8,128)(2,1)} %x_hbm.1, bf16[1024,512]{1,0:T(8,128)(2,1)} %qc_hbm.1, bf16[1024,512]{1,0:T(8,128)(2,1)} %kc_hbm.1, ...), custom_call_target="tpu_custom_call" | custom-call | tf_op jit(solution)/shard_map/exchange/pallas_call | solution.py:702
  89.5 6.1 %final.1 = (f32[1024,512]{1,0:T(8,128)}, f32[1024,512]{1,0:T(8,128)}, bf16[4096,512]{1,0:T(8,128)(2,1)}, f32[64,512]{1,0:T(8,128)}, f32[64,512]{1,0:T(8,128)}, /...) custom-call(f32[2,64,512]{2,1,0:T(8,128)S(1)} %get-tuple-element.15., ...), custom_call_target="tpu_custom_call" | custom-call | tf_op jit(solution)/shard_map/final/pallas_call | solution.py:739

commit v4 on v3

--- a/solution.py
+++ b/solution.py
@@ -58,6 +58,7 @@
     ratio,
     sums,
     scales,
+    changes,
     load_sem,
     b_send,
     b_recv,
@@ -196,6 +197,17 @@
 
     loads[0].wait()
     loads[1].wait()
+    early = z < depth // 2
+
+    def round_masters():
+        for j in range(2):
+            loads[2 + j].wait()
+
+            @pl.loop(0, pieces)
+            def _(i, j=j):
+                gathered[j, at(f * rows + i * tile, tile), :] = master[j, at(i * tile, tile), :].astype(BF)
+
+    pl.when(early)(round_masters)
     pl.semaphore_wait(barrier, fs - 1 + depth)
     if relay:
 
@@ -213,13 +225,7 @@
                     for h in range(2):
                         basis_copy(m, j, h, f ^ m).start()
 
-    for j in range(2):
-        loads[2 + j].wait()
-
-        @pl.loop(0, pieces)
-        def _(i, j=j):
-            gathered[j, at(f * rows + i * tile, tile), :] = master[j, at(i * tile, tile), :].astype(BF)
-
+    pl.when(jnp.logical_not(early))(round_masters)
     if relay:
         first_marks = [[count * k // 24 for k in pair] for pair in FIRST]
 
@@ -590,9 +596,13 @@
 
         @pl.loop(0, rows // pair)
         def _(i):
-            for m in (2, 1):
-                relay_wait(m, i)
-                finish_rows(2 - m, (f ^ 3) * rows + i * pair, pair)
+            place = at((f ^ 3) * rows + i * pair, pair)
+            for j in range(2):
+                update = jnp.dot(basis[j, place, :], ratio[j], preferred_element_type=F32)
+                changes[j] = update * (step_rate * scales[j, 0:1, :])
+            for j in range(2):
+                relay_wait(2 - j, i)
+                copy_ref[j, place, :] = (gathered[j, place, :].astype(F32) - changes[j]).astype(BF)
     else:
         for m in range(1, fs):
             for j in range(2):
@@ -725,6 +735,7 @@
             pltpu.VMEM((2, rank, width), BF),
             pltpu.VMEM((fs, -(-2 * width // HD // 8) * 8, HD), F32),
             pltpu.VMEM((2, 8, width), F32),
+            pltpu.VMEM((2, min(rows, 256), width), F32),
             dma((7,)),
             *pairs,
         ],

time: 95.9 us -> 95.2 us (level)
  no operation moved by 1% of the time
where the time goes in v4:
time: 95.2 us; the launch traced here: 95.1 us
  Pallas kernels  94.4 us (99%)
    pallas_call x1, Pallas kernels, body(): pl.pallas_call(functools.partial(exchange_kernel, fs, tp), name='exchange...  88.3 us
    pallas_call x1, Pallas kernels, body(): pl.pallas_call(final_kernel, name='final', out_shape=(big, big, copied, s...  6.09 us

profile of v4, /device:TPU:0, one launch (start us, length us, event | category | flops | bytes accessed | tf_op | source)
XLA Modules:
  0.0 95.1 jit_solution(8448602082048641533)
XLA Ops:
  0.6 88.3 %exchange.1 = (f32[2,64,512]{2,1,0:T(8,128)S(1)}, f32[2,64,512]{2,1,0:T(8,128)S(1)}, f32[2,1024,512]{2,1,0:T(8,128)S(1)}, f32[2,1024,512]{2,1,0:T(8,128)S(1)}, bf16[2,4096,512]{2,1,0:T(8,128)(2,1)S(1)}) custom-call(bf16[1024,512]{1,0:T(8,128)(2,1)} %x_hbm.1, bf16[1024,512]{1,0:T(8,128)(2,1)} %qc_hbm.1, bf16[1024,512]{1,0:T(8,128)(2,1)} %kc_hbm.1, ...), custom_call_target="tpu_custom_call" | custom-call | tf_op jit(solution)/shard_map/exchange/pallas_call | solution.py:712
  89.0 6.1 %final.1 = (f32[1024,512]{1,0:T(8,128)}, f32[1024,512]{1,0:T(8,128)}, bf16[4096,512]{1,0:T(8,128)(2,1)}, f32[64,512]{1,0:T(8,128)}, f32[64,512]{1,0:T(8,128)}, /...) custom-call(f32[2,64,512]{2,1,0:T(8,128)S(1)} %get-tuple-element.15., ...), custom_call_target="tpu_custom_call" | custom-call | tf_op jit(solution)/shard_map/final/pallas_call | solution.py:750

commit v5 on v4

--- a/solution.py
+++ b/solution.py
@@ -672,6 +672,7 @@
     for j in range(2):
         for k, source in enumerate((step, weight, copy, first, second)):
             moves.append((source.at[j], outs[5 * j + k]))
+    moves.sort(key=lambda move: -move[0].size)
     moves = [pltpu.make_async_copy(a, b, sem.at[i]) for i, (a, b) in enumerate(moves)]
     for move in moves:
         move.start()

time: 95.2 us -> 95.2 us (level)
  no operation moved by 1% of the time
where the time goes in v5:
time: 95.2 us; the launch traced here: 95 us
  Pallas kernels  94.4 us (99%)
    pallas_call x1, Pallas kernels, body(): pl.pallas_call(functools.partial(exchange_kernel, fs, tp), name='exchange...  88.3 us
    pallas_call x1, Pallas kernels, body(): pl.pallas_call(final_kernel, name='final', out_shape=(big, big, copied, s...  6.03 us

profile of v5, /device:TPU:0, one launch (start us, length us, event | category | flops | bytes accessed | tf_op | source)
XLA Modules:
  0.0 95.0 jit_solution(5915659493996815217)
XLA Ops:
  0.6 88.3 %exchange.1 = (f32[2,64,512]{2,1,0:T(8,128)S(1)}, f32[2,64,512]{2,1,0:T(8,128)S(1)}, f32[2,1024,512]{2,1,0:T(8,128)S(1)}, f32[2,1024,512]{2,1,0:T(8,128)S(1)}, bf16[2,4096,512]{2,1,0:T(8,128)(2,1)S(1)}) custom-call(bf16[1024,512]{1,0:T(8,128)(2,1)} %x_hbm.1, bf16[1024,512]{1,0:T(8,128)(2,1)} %qc_hbm.1, bf16[1024,512]{1,0:T(8,128)(2,1)} %kc_hbm.1, ...), custom_call_target="tpu_custom_call" | custom-call | tf_op jit(solution)/shard_map/exchange/pallas_call | solution.py:713
  89.0 6.0 %final.1 = (f32[1024,512]{1,0:T(8,128)}, f32[1024,512]{1,0:T(8,128)}, bf16[4096,512]{1,0:T(8,128)(2,1)}, f32[64,512]{1,0:T(8,128)}, f32[64,512]{1,0:T(8,128)}, /...) custom-call(f32[2,64,512]{2,1,0:T(8,128)S(1)} %get-tuple-element.15., ...), custom_call_target="tpu_custom_call" | custom-call | tf_op jit(solution)/shard_map/final/pallas_call | solution.py:751
